TPU v7x, 32 devices: a whole 2x2x4 slice. The times are simulated.
32 devices in a mesh: ep: 8 (over z, core), tp: 4 (over y, x).
Axes of the slice: x: 2, y: 2, z: 4, core: 2. Of those that a mesh axis runs over, the one named last changes fastest.
Arguments:
- query_in: bfloat16 [1024, 8192], P('tp', 'ep'), may hold values from -6 to 6
- key_in: bfloat16 [1024, 8192], P('tp', 'ep'), may hold values from -10 to 10
- value_in: bfloat16 [1024, 8192], P('tp', 'ep'), may hold values from -6 to 6
- erase_pre: bfloat16 [1024, 8192], P('tp', 'ep'), may hold values from -8 to 5
- decay_pre: bfloat16 [1024, 8192], P('tp', 'ep'), may hold values from -30 to 4.5
- mix_gain: float32 [1024], P('tp'), may hold values from 0.1 to 1.9
- expert_in: bfloat16 [2048, 2048], P('ep'), may hold values from -6 to 6
- expert_gain: float32 [2048], replicated, may hold values from 0.1 to 1.9
- routes: int32 [2048, 2], P('ep'), may hold values from 0 to 7, all different within a row; in each aligned block of 256 rows (0 to 255, 256 to 511, ...) at most 96 rows name the same one
- route_weight: float32 [2048, 2], P('ep'), may hold values from 0.1 to 1
- gate_weight: bfloat16 [8, 2048, 3584], P('ep', None, 'tp'), may hold values from -0.125 to 0.125
- up_weight: bfloat16 [8, 2048, 3584], P('ep', None, 'tp'), may hold values from -0.125 to 0.125
- down_weight: bfloat16 [8, 3584, 2048], P('ep', 'tp'), may hold values from -0.09375 to 0.09375
Outputs:
- mixer_out: bfloat16 [1024, 8192], P('tp', 'ep')
- expert_out: bfloat16 [2048, 2048], P('ep', 'tp')
Inputs may be any that keep to these rules, and one draw needn't show every extreme that they name: `routes`: A row's 2 experts differ. Within the 256 rows of one index of ep, every expert is named at most 96 times; in some of these aligned blocks one expert is named exactly 96 times.
All inputs are finite; a program needn't handle non-finite values.
Results may differ from a plain program's by a relative error of at most 0.015.
Values may be sent and summed in bfloat16 or wider, within the bound.
A program may use at most 128 MiB of HBM per device.

v0:
```python
import jax
import jax.numpy as jnp
from jax import lax
from jax.sharding import PartitionSpec as P

HEAD_DIM = 64
BLOCK_TOKENS = 64


highest = lax.Precision.HIGHEST


def prefix(array, axis, combine, identity, reverse):
    count, mine = (lax.axis_size(axis), lax.axis_index(axis))
    everything = jax.tree.map(
        lambda part, kind: lax.all_gather(part.astype(kind), axis),
        array,
        jax.tree.map(lambda a: jnp.bfloat16 if a.dtype == jnp.float32 else a.dtype, array),
    )
    start = jax.tree.map(
        lambda part, zero: jnp.broadcast_to(jnp.asarray(zero, part.dtype), part.shape),
        array,
        identity,
    )

    def lap(k, before):
        at = count - 1 - k if reverse else k
        reached = at > mine if reverse else at < mine
        new = combine(
            before, jax.tree.map(lambda part, own: part[at].astype(own.dtype), everything, array)
        )
        return jax.tree.map(lambda a, b: jnp.where(reached, a, b), new, before)

    return lax.fori_loop(0, count, lap, start)


def token_terms(key_in, erase_pre, decay_pre):
    key_f = key_in.astype(jnp.float32)
    unit_key = key_f * lax.rsqrt(jnp.sum(key_f * key_f, axis=-1, keepdims=True) + 1e-05)
    eraser = unit_key * jax.nn.sigmoid(erase_pre.astype(jnp.float32))
    log_keep = -jnp.exp(-jax.nn.softplus(-decay_pre.astype(jnp.float32)) - 0.5)
    return (key_f, unit_key, eraser, log_keep)


def paired(left, right, mask):
    return jnp.where(mask, jnp.einsum("nthk,nshk->nhts", left, right, precision=highest), 0.0)


def run_blocks(terms):
    query_f, key_f, value_f, unit_key, eraser, log_keep = terms
    block_count, span, head_count, channels = query_f.shape
    cumulative = jnp.cumsum(log_keep, axis=1)
    prior_cum = cumulative - log_keep
    last_cum = cumulative[:, -1:]
    growth = jnp.exp(-cumulative)
    key_up = key_f * growth
    erase_up = eraser * growth
    unit_down = unit_key * jnp.exp(prior_cum)
    query_down = query_f * jnp.exp(cumulative)
    fade = jnp.exp(last_cum - cumulative)
    key_end = key_f * fade
    erase_end = eraser * fade
    position = jnp.arange(span)
    strict = position[:, None] > position[None, :]
    inclusive = position[:, None] >= position[None, :]
    key_mix = paired(unit_down, key_up, strict)
    erase_mix = paired(unit_down, erase_up, strict)
    key_read = paired(query_down, key_up, inclusive)
    erase_read = paired(query_down, erase_up, inclusive)
    solve_mat = erase_mix + jnp.eye(span, dtype=jnp.float32)
    augmented = jnp.concatenate([value_f, jnp.zeros_like(value_f)], axis=-1)
    decay_end = jnp.exp(last_cum[:, 0])
    identity_rows = jnp.broadcast_to(
        jnp.eye(channels, dtype=jnp.float32), (head_count, channels, channels)
    )
    initial = jnp.concatenate([jnp.zeros_like(identity_rows), identity_rows], axis=1)

    def advance(carried, block):
        (
            unit_b,
            query_b,
            key_end_b,
            erase_end_b,
            value_b,
            kmix_b,
            smat_b,
            kread_b,
            eread_b,
            decay_b,
        ) = block
        right_side = jnp.einsum("hvk,thk->htv", carried, unit_b, precision=highest) + jnp.einsum(
            "hts,shv->htv", kmix_b, value_b, precision=highest
        )
        removed = jax.scipy.linalg.solve_triangular(
            smat_b, right_side, lower=True, unit_diagonal=True
        )
        readout = (
            jnp.einsum("hvk,thk->thv", carried, query_b, precision=highest)
            + jnp.einsum("hts,shv->thv", kread_b, value_b, precision=highest)
            - jnp.einsum("hts,hsv->thv", eread_b, removed, precision=highest)
        )
        updated = (
            carried * decay_b[:, None, :]
            + jnp.einsum("shv,shk->hvk", value_b, key_end_b, precision=highest)
            - jnp.einsum("hsv,shk->hvk", removed, erase_end_b, precision=highest)
        )
        return (updated, readout)

    final, readouts = lax.scan(
        advance,
        initial,
        (
            unit_down,
            query_down,
            key_end,
            erase_end,
            augmented,
            key_mix,
            solve_mat,
            key_read,
            erase_read,
            decay_end,
        ),
    )
    return (readouts.reshape(block_count * span, head_count, 2 * channels), final)


def compose(earlier, later):
    return (
        jnp.einsum("hij,hjk->hik", earlier[0], later[0], precision=highest),
        jnp.einsum("hvj,hjk->hvk", earlier[1], later[0], precision=highest) + later[1],
    )


def mixer_half(query_in, key_in, value_in, erase_pre, decay_pre, mix_gain):
    seq_len = query_in.shape[0]
    head_count = query_in.shape[1] // HEAD_DIM
    layout = (seq_len // BLOCK_TOKENS, BLOCK_TOKENS, head_count, HEAD_DIM)
    query_f = query_in.astype(jnp.float32).reshape(layout)
    value_f = value_in.astype(jnp.float32).reshape(layout)
    key_f, unit_key, eraser, log_keep = token_terms(
        key_in.reshape(layout), erase_pre.reshape(layout), decay_pre.reshape(layout)
    )
    terms = (query_f, key_f, value_f, unit_key, eraser, log_keep)
    ahead_read, ahead_end = run_blocks(terms)
    flipped = tuple(
        (jnp.flip(item.reshape(seq_len, head_count, HEAD_DIM), 0).reshape(layout) for item in terms)
    )
    behind_read, behind_end = run_blocks(flipped)
    behind_read = jnp.flip(behind_read, 0)
    ahead_maps = (ahead_end[:, HEAD_DIM:, :], ahead_end[:, :HEAD_DIM, :])
    behind_maps = (behind_end[:, HEAD_DIM:, :], behind_end[:, :HEAD_DIM, :])
    empty_state = jnp.zeros((head_count, HEAD_DIM, HEAD_DIM), jnp.float32)
    identity_maps = (
        jnp.broadcast_to(jnp.eye(HEAD_DIM, dtype=jnp.float32), (head_count, HEAD_DIM, HEAD_DIM)),
        empty_state,
    )
    enter_ahead = prefix(ahead_maps, "ep", compose, identity_maps, False)[1]
    enter_behind = prefix(behind_maps, "ep", compose, identity_maps, True)[1]
    summed = (
        ahead_read[..., :HEAD_DIM]
        + jnp.einsum("hvk,thk->thv", enter_ahead, ahead_read[..., HEAD_DIM:], precision=highest)
        + behind_read[..., :HEAD_DIM]
        + jnp.einsum("hvk,thk->thv", enter_behind, behind_read[..., HEAD_DIM:], precision=highest)
    )
    center = jnp.mean(summed, axis=-1, keepdims=True)
    spread = jnp.mean(jnp.square(summed - center), axis=-1, keepdims=True)
    scaled = (
        (summed - center)
        * lax.rsqrt(spread + HEAD_DIM * 1e-05)
        * mix_gain.reshape(head_count, HEAD_DIM)
    )
    return scaled.astype(jnp.bfloat16).reshape(seq_len, head_count * HEAD_DIM)


def slot_targets(routes, experts_n, capacity):
    onehot = (routes[:, :, None] == jnp.arange(experts_n, dtype=jnp.int32)[None, None, :]).astype(
        jnp.int32
    )
    flat = onehot.reshape(-1, experts_n)
    before = jnp.cumsum(flat, axis=0) - flat
    slot_index = jnp.sum(before * flat, axis=-1).reshape(routes.shape)
    return routes * capacity + slot_index


def dispatch_matrix(targets, slot_total):
    matches = targets[None, :, :] == jnp.arange(slot_total, dtype=jnp.int32)[:, None, None]
    return jnp.sum(matches.astype(jnp.float32), axis=-1).astype(jnp.bfloat16)


def expert_half(expert_in, expert_gain, routes, route_weight, gate_weight, up_weight, down_weight):
    experts_n = lax.axis_size("ep")
    row_count = expert_in.shape[0]
    capacity = 3 * routes.shape[1] * row_count // (2 * experts_n)
    slot_total = experts_n * capacity
    input_f = expert_in.astype(jnp.float32)
    normed = (
        input_f
        * lax.rsqrt(jnp.mean(input_f * input_f, axis=-1, keepdims=True) + 1e-06)
        * expert_gain
    ).astype(jnp.bfloat16)
    targets = slot_targets(routes, experts_n, capacity)
    buffer = jnp.dot(
        dispatch_matrix(targets, slot_total), normed, preferred_element_type=jnp.float32
    ).astype(jnp.bfloat16)
    gate_local = gate_weight[0]
    up_local = up_weight[0]
    down_local = down_weight[0]
    col_count = normed.shape[1] // lax.axis_size("tp")
    arrived = lax.all_to_all(
        buffer.reshape(experts_n, capacity, normed.shape[1]),
        "ep",
        split_axis=0,
        concat_axis=0,
        tiled=True,
    ).reshape(slot_total, normed.shape[1])
    gate_sum = jnp.dot(arrived, gate_local, preferred_element_type=jnp.float32)
    up_sum = jnp.dot(arrived, up_local, preferred_element_type=jnp.float32)
    hidden = (jax.nn.silu(gate_sum) * up_sum).astype(jnp.bfloat16)
    summed = lax.psum_scatter(
        lax.dot_general(
            down_local, hidden, (((0,), (1,)), ((), ())), preferred_element_type=jnp.float32
        ).astype(jnp.bfloat16),
        "tp",
        scatter_dimension=0,
        tiled=True,
    )
    returned = lax.all_to_all(
        summed.reshape(col_count, experts_n, capacity),
        "ep",
        split_axis=1,
        concat_axis=1,
        tiled=True,
    ).reshape(col_count, slot_total)
    matches = targets[:, :, None] == jnp.arange(slot_total, dtype=jnp.int32)[None, None, :]
    combine = jnp.sum(matches.astype(jnp.float32) * route_weight[:, :, None], axis=1)
    return jnp.einsum("tx,cx->tc", combine, returned.astype(jnp.float32), precision=highest).astype(
        jnp.bfloat16
    )


def on_device(
    query_in,
    key_in,
    value_in,
    erase_pre,
    decay_pre,
    mix_gain,
    expert_in,
    expert_gain,
    routes,
    route_weight,
    gate_weight,
    up_weight,
    down_weight,
):
    mixer_out = mixer_half(query_in.T, key_in.T, value_in.T, erase_pre.T, decay_pre.T, mix_gain).T
    expert_out = expert_half(
        expert_in, expert_gain, routes, route_weight, gate_weight, up_weight, down_weight
    )
    return (mixer_out, expert_out)


def solution(mesh):
    placed = (
        P("tp", "ep"),
        P("tp", "ep"),
        P("tp", "ep"),
        P("tp", "ep"),
        P("tp", "ep"),
        P("tp"),
        P("ep", None),
        P(),
        P("ep", None),
        P("ep", None),
        P("ep", None, "tp"),
        P("ep", None, "tp"),
        P("ep", "tp", None),
    )
    return jax.shard_map(
        on_device,
        mesh=mesh,
        in_specs=placed,
        out_specs=(P("tp", "ep"), P("ep", "tp")),
        check_vma=False,
    )
```

profile of v0, /device:TPU:0, one launch (start us, length us, event | category | flops | bytes accessed | tf_op | source)
XLA Modules:
  0.0 1431.7 jit_solution(7739347053799351243)
XLA Ops:
  199.9 547.2 %while.55 = (s32[]{:T(128)}, f32[4,128,64]{1,2,0:T(8,128)S(1)}, f32[16,64,4,128]{3,1,0,2:T(8,128)S(1)}, f32[16,4,64]{2,0,1:T(8,128)}, f32[16,64,4,128]{3,1,2,0:T...) while((s32[]{:T(128)}, f32[4,128,64]{1,2,0:T(8,128)S(1)}, ...), condition=%wide.region_8.10_spmd, body=%wide.region_7.9_spmd.sunk | while | flops 201568320 | bytes 4046993 | solution.py:109
  204.2 21.0 %custom-call.11 = f32[4,1,64,64]{2,3,1,0:T(8,128)} custom-call(f32[4,1,64,64]{3,2,1,0:T(8,128)} %fusion.304), custom_call_target="InvertDiagBlocksLowerTriangular" | custom-call | tf_op jit(solution)/shard_map/while/body/eval_jaxpr/jit(_solve_triangular)/vmap()/triangular_solve | solution.py:94
  238.4 21.0 %custom-call.11 = f32[4,1,64,64]{2,3,1,0:T(8,128)} custom-call(f32[4,1,64,64]{3,2,1,0:T(8,128)} %fusion.304), custom_call_target="InvertDiagBlocksLowerTriangular" | custom-call | tf_op jit(solution)/shard_map/while/body/eval_jaxpr/jit(_solve_triangular)/vmap()/triangular_solve | solution.py:94
  272.6 21.0 %custom-call.11 = f32[4,1,64,64]{2,3,1,0:T(8,128)} custom-call(f32[4,1,64,64]{3,2,1,0:T(8,128)} %fusion.304), custom_call_target="InvertDiagBlocksLowerTriangular" | custom-call | tf_op jit(solution)/shard_map/while/body/eval_jaxpr/jit(_solve_triangular)/vmap()/triangular_solve | solution.py:94
  306.8 21.0 %custom-call.11 = f32[4,1,64,64]{2,3,1,0:T(8,128)} custom-call(f32[4,1,64,64]{3,2,1,0:T(8,128)} %fusion.304), custom_call_target="InvertDiagBlocksLowerTriangular" | custom-call | tf_op jit(solution)/shard_map/while/body/eval_jaxpr/jit(_solve_triangular)/vmap()/triangular_solve | solution.py:94
  341.0 21.0 %custom-call.11 = f32[4,1,64,64]{2,3,1,0:T(8,128)} custom-call(f32[4,1,64,64]{3,2,1,0:T(8,128)} %fusion.304), custom_call_target="InvertDiagBlocksLowerTriangular" | custom-call | tf_op jit(solution)/shard_map/while/body/eval_jaxpr/jit(_solve_triangular)/vmap()/triangular_solve | solution.py:94
  375.2 21.0 %custom-call.11 = f32[4,1,64,64]{2,3,1,0:T(8,128)} custom-call(f32[4,1,64,64]{3,2,1,0:T(8,128)} %fusion.304), custom_call_target="InvertDiagBlocksLowerTriangular" | custom-call | tf_op jit(solution)/shard_map/while/body/eval_jaxpr/jit(_solve_triangular)/vmap()/triangular_solve | solution.py:94
  409.4 21.0 %custom-call.11 = f32[4,1,64,64]{2,3,1,0:T(8,128)} custom-call(f32[4,1,64,64]{3,2,1,0:T(8,128)} %fusion.304), custom_call_target="InvertDiagBlocksLowerTriangular" | custom-call | tf_op jit(solution)/shard_map/while/body/eval_jaxpr/jit(_solve_triangular)/vmap()/triangular_solve | solution.py:94
  443.6 21.0 %custom-call.11 = f32[4,1,64,64]{2,3,1,0:T(8,128)} custom-call(f32[4,1,64,64]{3,2,1,0:T(8,128)} %fusion.304), custom_call_target="InvertDiagBlocksLowerTriangular" | custom-call | tf_op jit(solution)/shard_map/while/body/eval_jaxpr/jit(_solve_triangular)/vmap()/triangular_solve | solution.py:94
  477.7 21.0 %custom-call.11 = f32[4,1,64,64]{2,3,1,0:T(8,128)} custom-call(f32[4,1,64,64]{3,2,1,0:T(8,128)} %fusion.304), custom_call_target="InvertDiagBlocksLowerTriangular" | custom-call | tf_op jit(solution)/shard_map/while/body/eval_jaxpr/jit(_solve_triangular)/vmap()/triangular_solve | solution.py:94
  511.9 21.0 %custom-call.11 = f32[4,1,64,64]{2,3,1,0:T(8,128)} custom-call(f32[4,1,64,64]{3,2,1,0:T(8,128)} %fusion.304), custom_call_target="InvertDiagBlocksLowerTriangular" | custom-call | tf_op jit(solution)/shard_map/while/body/eval_jaxpr/jit(_solve_triangular)/vmap()/triangular_solve | solution.py:94
  546.1 21.0 %custom-call.11 = f32[4,1,64,64]{2,3,1,0:T(8,128)} custom-call(f32[4,1,64,64]{3,2,1,0:T(8,128)} %fusion.304), custom_call_target="InvertDiagBlocksLowerTriangular" | custom-call | tf_op jit(solution)/shard_map/while/body/eval_jaxpr/jit(_solve_triangular)/vmap()/triangular_solve | solution.py:94
  580.3 21.0 %custom-call.11 = f32[4,1,64,64]{2,3,1,0:T(8,128)} custom-call(f32[4,1,64,64]{3,2,1,0:T(8,128)} %fusion.304), custom_call_target="InvertDiagBlocksLowerTriangular" | custom-call | tf_op jit(solution)/shard_map/while/body/eval_jaxpr/jit(_solve_triangular)/vmap()/triangular_solve | solution.py:94
  614.5 21.0 %custom-call.11 = f32[4,1,64,64]{2,3,1,0:T(8,128)} custom-call(f32[4,1,64,64]{3,2,1,0:T(8,128)} %fusion.304), custom_call_target="InvertDiagBlocksLowerTriangular" | custom-call | tf_op jit(solution)/shard_map/while/body/eval_jaxpr/jit(_solve_triangular)/vmap()/triangular_solve | solution.py:94
  648.7 21.0 %custom-call.11 = f32[4,1,64,64]{2,3,1,0:T(8,128)} custom-call(f32[4,1,64,64]{3,2,1,0:T(8,128)} %fusion.304), custom_call_target="InvertDiagBlocksLowerTriangular" | custom-call | tf_op jit(solution)/shard_map/while/body/eval_jaxpr/jit(_solve_triangular)/vmap()/triangular_solve | solution.py:94
  682.9 21.0 %custom-call.11 = f32[4,1,64,64]{2,3,1,0:T(8,128)} custom-call(f32[4,1,64,64]{3,2,1,0:T(8,128)} %fusion.304), custom_call_target="InvertDiagBlocksLowerTriangular" | custom-call | tf_op jit(solution)/shard_map/while/body/eval_jaxpr/jit(_solve_triangular)/vmap()/triangular_solve | solution.py:94
  717.1 21.0 %custom-call.11 = f32[4,1,64,64]{2,3,1,0:T(8,128)} custom-call(f32[4,1,64,64]{3,2,1,0:T(8,128)} %fusion.304), custom_call_target="InvertDiagBlocksLowerTriangular" | custom-call | tf_op jit(solution)/shard_map/while/body/eval_jaxpr/jit(_solve_triangular)/vmap()/triangular_solve | solution.py:94
  756.6 511.0 %while.54 = (s32[]{:T(128)}, f32[4,128,64]{1,2,0:T(8,128)S(1)}, f32[16,64,4,128]{3,1,0,2:T(8,128)}, f32[16,4,64]{2,0,1:T(8,128)}, f32[16,64,4,128]{3,1,2,0:T(8,1...) while((s32[]{:T(128)}, f32[4,128,64]{1,2,0:T(8,128)S(1)}, ...), condition=%wide.region_3.5_spmd, body=%wide.region_2.4_spmd.sunk | while | flops 201568320 | bytes 4046993 | solution.py:109
  792.0 19.7 %custom-call.10 = f32[4,1,64,64]{2,3,1,0:T(8,128)S(1)} custom-call(f32[4,1,64,64]{3,2,1,0:T(8,128)S(1)} %fusion.284), custom_call_target="InvertDiagBlocksLowerTriangular" | custom-call | tf_op jit(solution)/shard_map/while/body/eval_jaxpr/jit(_solve_triangular)/vmap()/triangular_solve | solution.py:94
  855.9 19.7 %custom-call.10 = f32[4,1,64,64]{2,3,1,0:T(8,128)S(1)} custom-call(f32[4,1,64,64]{3,2,1,0:T(8,128)S(1)} %fusion.284), custom_call_target="InvertDiagBlocksLowerTriangular" | custom-call | tf_op jit(solution)/shard_map/while/body/eval_jaxpr/jit(_solve_triangular)/vmap()/triangular_solve | solution.py:94
  887.8 19.7 %custom-call.10 = f32[4,1,64,64]{2,3,1,0:T(8,128)S(1)} custom-call(f32[4,1,64,64]{3,2,1,0:T(8,128)S(1)} %fusion.284), custom_call_target="InvertDiagBlocksLowerTriangular" | custom-call | tf_op jit(solution)/shard_map/while/body/eval_jaxpr/jit(_solve_triangular)/vmap()/triangular_solve | solution.py:94
  919.8 19.7 %custom-call.10 = f32[4,1,64,64]{2,3,1,0:T(8,128)S(1)} custom-call(f32[4,1,64,64]{3,2,1,0:T(8,128)S(1)} %fusion.284), custom_call_target="InvertDiagBlocksLowerTriangular" | custom-call | tf_op jit(solution)/shard_map/while/body/eval_jaxpr/jit(_solve_triangular)/vmap()/triangular_solve | solution.py:94
  951.7 19.7 %custom-call.10 = f32[4,1,64,64]{2,3,1,0:T(8,128)S(1)} custom-call(f32[4,1,64,64]{3,2,1,0:T(8,128)S(1)} %fusion.284), custom_call_target="InvertDiagBlocksLowerTriangular" | custom-call | tf_op jit(solution)/shard_map/while/body/eval_jaxpr/jit(_solve_triangular)/vmap()/triangular_solve | solution.py:94
  983.7 19.7 %custom-call.10 = f32[4,1,64,64]{2,3,1,0:T(8,128)S(1)} custom-call(f32[4,1,64,64]{3,2,1,0:T(8,128)S(1)} %fusion.284), custom_call_target="InvertDiagBlocksLowerTriangular" | custom-call | tf_op jit(solution)/shard_map/while/body/eval_jaxpr/jit(_solve_triangular)/vmap()/triangular_solve | solution.py:94
  1015.6 19.7 %custom-call.10 = f32[4,1,64,64]{2,3,1,0:T(8,128)S(1)} custom-call(f32[4,1,64,64]{3,2,1,0:T(8,128)S(1)} %fusion.284), custom_call_target="InvertDiagBlocksLowerTriangular" | custom-call | tf_op jit(solution)/shard_map/while/body/eval_jaxpr/jit(_solve_triangular)/vmap()/triangular_solve | solution.py:94
  1047.6 19.7 %custom-call.10 = f32[4,1,64,64]{2,3,1,0:T(8,128)S(1)} custom-call(f32[4,1,64,64]{3,2,1,0:T(8,128)S(1)} %fusion.284), custom_call_target="InvertDiagBlocksLowerTriangular" | custom-call | tf_op jit(solution)/shard_map/while/body/eval_jaxpr/jit(_solve_triangular)/vmap()/triangular_solve | solution.py:94
  1079.5 19.7 %custom-call.10 = f32[4,1,64,64]{2,3,1,0:T(8,128)S(1)} custom-call(f32[4,1,64,64]{3,2,1,0:T(8,128)S(1)} %fusion.284), custom_call_target="InvertDiagBlocksLowerTriangular" | custom-call | tf_op jit(solution)/shard_map/while/body/eval_jaxpr/jit(_solve_triangular)/vmap()/triangular_solve | solution.py:94
  1111.4 19.7 %custom-call.10 = f32[4,1,64,64]{2,3,1,0:T(8,128)S(1)} custom-call(f32[4,1,64,64]{3,2,1,0:T(8,128)S(1)} %fusion.284), custom_call_target="InvertDiagBlocksLowerTriangular" | custom-call | tf_op jit(solution)/shard_map/while/body/eval_jaxpr/jit(_solve_triangular)/vmap()/triangular_solve | solution.py:94
  1143.4 19.7 %custom-call.10 = f32[4,1,64,64]{2,3,1,0:T(8,128)S(1)} custom-call(f32[4,1,64,64]{3,2,1,0:T(8,128)S(1)} %fusion.284), custom_call_target="InvertDiagBlocksLowerTriangular" | custom-call | tf_op jit(solution)/shard_map/while/body/eval_jaxpr/jit(_solve_triangular)/vmap()/triangular_solve | solution.py:94
  1175.3 19.7 %custom-call.10 = f32[4,1,64,64]{2,3,1,0:T(8,128)S(1)} custom-call(f32[4,1,64,64]{3,2,1,0:T(8,128)S(1)} %fusion.284), custom_call_target="InvertDiagBlocksLowerTriangular" | custom-call | tf_op jit(solution)/shard_map/while/body/eval_jaxpr/jit(_solve_triangular)/vmap()/triangular_solve | solution.py:94
  1207.2 19.7 %custom-call.10 = f32[4,1,64,64]{2,3,1,0:T(8,128)S(1)} custom-call(f32[4,1,64,64]{3,2,1,0:T(8,128)S(1)} %fusion.284), custom_call_target="InvertDiagBlocksLowerTriangular" | custom-call | tf_op jit(solution)/shard_map/while/body/eval_jaxpr/jit(_solve_triangular)/vmap()/triangular_solve | solution.py:94
  1239.2 19.7 %custom-call.10 = f32[4,1,64,64]{2,3,1,0:T(8,128)S(1)} custom-call(f32[4,1,64,64]{3,2,1,0:T(8,128)S(1)} %fusion.284), custom_call_target="InvertDiagBlocksLowerTriangular" | custom-call | tf_op jit(solution)/shard_map/while/body/eval_jaxpr/jit(_solve_triangular)/vmap()/triangular_solve | solution.py:94
  (640 shorter events, 828.5 us)
Async XLA Ops:
  7.2 5.5 copy-start.8
  7.2 5.5 copy-start.16
  15.5 6.7 copy-start.11
  15.5 1255.0 %all-to-all-start = ((bf16[8,96,2048]{2,1,0:T(8,128)(2,1)}), bf16[8,96,2048]{2,1,0:T(8,128)(2,1)}, u32[]{:S(2)}, u32[]{:S(2)}) async-start(bf16[8,96,2048]{2,1,0:T(8,128)(2,1)} %bitcast.58), calls=%async_computation | async-start | bytes 6291456 | tf_op jit(solution)/shard_map/all_to_all | solution.py:210
  22.0 1371.1 %reduce-scatter.2.cloned.1.call-start = ((), (), s32[]{:S(2)}) async-start(), calls=%async_computation.3 | async-start | bytes 3932160 | tf_op jit(solution)/shard_map/reduce_scatter | solution.py:220
  29.7 3.7 copy-start.12
  35.0 4.8 copy-start.13
  76.7 3.5 copy-start.14
  104.2 2.0 copy-start.1
  112.4 6.4 copy-start
  125.1 6.4 copy-start.2
  131.5 2.4 copy-start.5
  138.4 2.9 copy-start.6
  140.0 1.3 copy-start.4
  143.2 3.5 copy-start.7
  185.8 3.5 copy-start.15
  1290.9 1.6 copy-start.3
  1393.1 28.8 %all-to-all-start.1 = ((bf16[512,8,96]{0,2,1:T(8,128)(2,1)}), bf16[512,8,96]{0,2,1:T(8,128)(2,1)}, u32[]{:S(2)}, u32[]{:S(2)}) async-start(bf16[512,8,96]{0,2,1:T(8,128)(2,1)} %bitcast.401), calls=%async_computation.2 | async-start | bytes 1572864 | tf_op jit(solution)/shard_map/all_to_all | solution.py:228
  1403.3 13.7 copy-start.18
  1403.3 13.8 copy-start.17
  1403.3 14.9 %copy-start.9 = (f32[1024,4,64]{0,2,1:T(8,128)S(1)}, f32[1024,4,64]{0,2,1:T(8,128)}, u32[]{:S(2)}) copy-start(f32[1024,4,64]{0,2,1:T(8,128)} %fusion.158) | copy-start | bytes 3145732
  1420.7 1.2 copy-start.10
Sparse Core Ops, SparseCore 0:
  1291.1 45.3 reduce-scatter.1
where the time goes:
time: 1450 us; the launch traced here: 1430 us
  other arithmetic  730 us (50%)
  matrix products  384 us (26%)
  local copies, waits for them, and re-layouts  225 us (16%)
  blocking collectives  63 us (4%)
  between operations  14.7 us (1%)
    another operation x128, other arithmetic, advance(): jax.scipy.linalg.solve_triangular(smat_b, right_side, lower=True, unit_di...  694 us
    dynamic_slice x64, local copies, waits for them, and re-layouts, run_blocks(): lax.scan(advance, initial, (unit_down, query_down, key_end, erase_end, au...  79.2 us
    all_gather x4, blocking collectives, prefix(): lax.all_gather(part.astype(kind), axis)  63 us
    dot_general x8, matrix products, paired(): jnp.einsum('nthk,nshk->nhts', left, right, precision=highest)  50.2 us
    dot_general x32, matrix products, advance(): jnp.einsum('hvk,thk->thv', carried, query_b, precision=highest)  48.1 us
    dot_general x32, matrix products, advance(): jnp.einsum('shv,shk->hvk', value_b, key_end_b, precision=highest)  41.2 us
    dot_general x32, matrix products, advance(): jnp.einsum('hts,shv->thv', kread_b, value_b, precision=highest)  39.6 us
    dot_general x32, matrix products, advance(): jnp.einsum('hts,shv->htv', kmix_b, value_b, precision=highest)  39.3 us
  transfers between devices with their start and end apart: 3, of which 0 were waited for; matrix products, arithmetic and copies ran while one was open for 91% of the time, Pallas kernels for 0%

commit v1 on v0

v1 whole, which is shorter than its diff:
```python
import math

import jax
import jax.numpy as jnp
from jax import lax
from jax.experimental import pallas as pl
from jax.experimental.pallas import tpu as pltpu
from jax.sharding import PartitionSpec as P

HEAD_DIM = 64


highest = lax.Precision.HIGHEST
SPAN = 128


def dot(left, right, dims=((1,), (0,)), precision=None):
    return lax.dot_general(
        left, right, (dims, ((), ())), precision=precision, preferred_element_type=jnp.float32
    )


def low(array):
    return array.astype(jnp.bfloat16)


TN = ((0,), (0,))
NT = ((1,), (1,))


def local_kernel(q_ref, k_ref, v_ref, e_ref, d_ref, read_ref, out_ref, step_ref, map_ref):
    channels, span = q_ref.shape
    heads = channels // HEAD_DIM
    row = lax.broadcasted_iota(jnp.int32, (span, span), 0)
    col = lax.broadcasted_iota(jnp.int32, (span, span), 1)
    crossed = row ^ col

    query_f = q_ref[...].astype(jnp.float32)
    key_f = k_ref[...].astype(jnp.float32)
    value = v_ref[...]
    log_keep = -math.exp(-0.5) / (1.0 + jnp.exp(-d_ref[...].astype(jnp.float32)))
    squares = (key_f * key_f).reshape(heads, HEAD_DIM, span)
    norm = lax.rsqrt(jnp.sum(squares, axis=1, keepdims=True) + 1e-05)
    unit = (key_f.reshape(heads, HEAD_DIM, span) * norm).reshape(channels, span)
    eraser = unit / (1.0 + jnp.exp(-e_ref[...].astype(jnp.float32)))

    upper = jnp.where(row <= col, 1.0, 0.0)
    cumulative = dot(log_keep, upper, precision=highest)
    prior = cumulative - log_keep
    total = cumulative[:, span - 1 :]
    middle = cumulative[:, span // 2 - 1 : span // 2]
    prior_up = jnp.exp(prior - middle)
    cum_down = jnp.exp(middle - cumulative)
    cum_up = jnp.exp(cumulative - middle)
    prior_down = jnp.exp(middle - prior)
    to_middle = jnp.exp(middle)
    from_middle = jnp.exp(total - middle)
    decay = jnp.exp(total)

    sides = (
        (unit * prior_up, query_f * cum_up, key_f * cum_down, eraser * cum_down,
         to_middle, from_middle, row < col, row <= col),
        (unit * cum_down, query_f * prior_down, key_f * prior_up, eraser * prior_up,
         from_middle, to_middle, row > col, row >= col),
    )
    units = []
    for side, (u, q, k, e, scale_in, scale_out, strict, inclusive) in enumerate(sides):
        u0, q0 = u * scale_in, q * scale_in
        for h in range(heads):
            at = slice(h * HEAD_DIM, (h + 1) * HEAD_DIM)
            uq = jnp.concatenate([low(u[at]), low(q[at])], axis=1)
            kb, eb = low(k[at]), low(e[at])
            mk = dot(kb, uq, TN)
            me = dot(eb, uq, TN)
            erase_mix = jnp.where(strict, me[:, :span], 0.0)
            units.append(
                dict(
                    side=side, h=h, at=at, kb=kb, eb=eb, u0=u0[at], q0=q0[at],
                    key_mix=low(jnp.where(strict, mk[:, :span], 0.0)),
                    key_read=low(jnp.where(inclusive, mk[:, span:], 0.0)),
                    erase_read=low(jnp.where(inclusive, me[:, span:], 0.0)),
                    erase_mix=erase_mix,
                    scale_out=scale_out[at], decay=decay[at],
                )
            )
    eye = jnp.where(row == col, 1.0, 0.0)
    solved = [eye - jnp.where(crossed == 1, m["erase_mix"], 0.0) for m in units]
    level = 1
    while (1 << level) < span:
        mask = (crossed >> level) == 1
        held = [low(x) for x in solved]
        half = [
            low(dot(x, low(jnp.where(mask, m["erase_mix"], 0.0)))) for x, m in zip(held, units)
        ]
        solved = [s - dot(y, x) for s, y, x in zip(solved, half, held)]
        level += 1

    outs = [None] * heads
    eye_k = jnp.where(
        lax.broadcasted_iota(jnp.int32, (HEAD_DIM, HEAD_DIM), 0)
        == lax.broadcasted_iota(jnp.int32, (HEAD_DIM, HEAD_DIM), 1),
        1.0,
        0.0,
    )
    for m, x in zip(units, solved):
        v = value[m["at"]]
        vm = dot(v, jnp.concatenate([m["key_mix"], m["key_read"]], axis=1))
        stacked = jnp.concatenate([low(vm[:, :span]), low(m["u0"])], axis=0)
        removed = low(dot(stacked, low(x)))
        taken = dot(removed, m["erase_read"])
        local = vm[:, span:] - taken[:HEAD_DIM]
        h, side = m["h"], m["side"]
        outs[h] = local if outs[h] is None else outs[h] + local
        read_ref[side, m["at"], :] = low(m["q0"] - taken[HEAD_DIM:])
        gone = dot(m["eb"], removed, NT)
        added = dot(m["kb"], v, NT)
        state = (added - gone[:, :HEAD_DIM]) * m["scale_out"]
        moved = eye_k * m["decay"] - gone[:, HEAD_DIM:] * m["scale_out"]
        step_ref[0, side, h] = jnp.concatenate([state, moved], axis=1)
    for h in range(heads):
        out_ref[h * HEAD_DIM : (h + 1) * HEAD_DIM, :] = outs[h]

    first = pl.program_id(0) == 0

    @pl.when(first)
    def _():
        map_ref[...] = step_ref[0]

    @pl.when(jnp.logical_not(first))
    def _():
        for h in range(heads):
            step = step_ref[0, 0, h]
            new = dot(step[:, HEAD_DIM:], map_ref[0, h], precision=highest)
            map_ref[0, h] = new + jnp.concatenate(
                [step[:, :HEAD_DIM], jnp.zeros_like(eye_k)], axis=1
            )
            before = map_ref[1, h]
            new = dot(before[:, HEAD_DIM:], step_ref[0, 1, h], precision=highest)
            map_ref[1, h] = new + jnp.concatenate(
                [before[:, :HEAD_DIM], jnp.zeros_like(eye_k)], axis=1
            )


def finish_kernel(maps_ref, step_ref, read_ref, local_ref, gain_ref, out_ref, enter_ref, states_ref):
    count = maps_ref.shape[0]
    heads = maps_ref.shape[2]
    blocks = step_ref.shape[0]
    mine = lax.axis_index("ep")
    enter_ref[...] = jnp.zeros_like(enter_ref)

    def gather(j, carry):
        for side, at in ((0, j), (1, count - 1 - j)):
            reached = at < mine if side == 0 else at > mine

            @pl.when(reached)
            def _():
                for h in range(heads):
                    part = maps_ref[at, side, h]
                    state = enter_ref[side, h]
                    high = low(state)
                    rest = low(state - high.astype(jnp.float32))
                    both = jnp.concatenate([high, rest], axis=1)
                    new = dot(part[:, HEAD_DIM:], both)
                    enter_ref[side, h] = (
                        new[:, :HEAD_DIM] + new[:, HEAD_DIM:] + part[:, :HEAD_DIM].astype(jnp.float32)
                    )

        return carry

    lax.fori_loop(0, count, gather, 0)

    def chain(j, carry):
        for side, at in ((0, j), (1, blocks - 1 - j)):
            for h in range(heads):
                step = step_ref[at, side, h]
                state = enter_ref[side, h]
                states_ref[at, h, side * HEAD_DIM : (side + 1) * HEAD_DIM, :] = low(state)
                enter_ref[side, h] = step[:, :HEAD_DIM] + dot(
                    step[:, HEAD_DIM:], state, precision=highest
                )
        return carry

    lax.fori_loop(0, blocks, chain, 0)

    def write(j, carry):
        tokens = pl.ds(pl.multiple_of(j * SPAN, SPAN), SPAN)
        for h in range(heads):
            at = slice(h * HEAD_DIM, (h + 1) * HEAD_DIM)
            reads = jnp.concatenate([read_ref[0, at, tokens], read_ref[1, at, tokens]], axis=0)
            summed = local_ref[at, tokens] + dot(states_ref[j, h], reads, TN)
            center = jnp.mean(summed, axis=0, keepdims=True)
            moved = summed - center
            spread = jnp.mean(moved * moved, axis=0, keepdims=True)
            scaled = moved * lax.rsqrt(spread + HEAD_DIM * 1e-05) * gain_ref[at, :]
            out_ref[at, tokens] = low(scaled)
        return carry

    lax.fori_loop(0, blocks, write, 0)


def mixer_half(query_in, key_in, value_in, erase_pre, decay_pre, mix_gain):
    channels, seq_len = query_in.shape
    heads = channels // HEAD_DIM
    blocks = seq_len // SPAN
    taken = pl.BlockSpec((channels, SPAN), lambda c: (0, c))
    f32 = jnp.float32
    reads, local, steps, maps = pl.pallas_call(
        local_kernel,
        grid=(blocks,),
        in_specs=[taken] * 5,
        out_specs=[
            pl.BlockSpec((2, channels, SPAN), lambda c: (0, 0, c)),
            taken,
            pl.BlockSpec((1, 2, heads, HEAD_DIM, 2 * HEAD_DIM), lambda c: (c, 0, 0, 0, 0)),
            pl.BlockSpec((2, heads, HEAD_DIM, 2 * HEAD_DIM), lambda c: (0, 0, 0, 0)),
        ],
        out_shape=[
            jax.ShapeDtypeStruct((2, channels, seq_len), jnp.bfloat16),
            jax.ShapeDtypeStruct((channels, seq_len), f32),
            jax.ShapeDtypeStruct((blocks, 2, heads, HEAD_DIM, 2 * HEAD_DIM), f32),
            jax.ShapeDtypeStruct((2, heads, HEAD_DIM, 2 * HEAD_DIM), f32),
        ],
        compiler_params=pltpu.CompilerParams(dimension_semantics=("arbitrary",)),
        cost_estimate=pl.CostEstimate(
            flops=int(4e10 * heads * blocks / 32), bytes_accessed=1 << 23, transcendentals=1 << 20
        ),
        name="mixer_local",
    )(query_in, key_in, value_in, erase_pre, decay_pre)
    gathered = lax.all_gather(maps.astype(jnp.bfloat16), "ep")
    return pl.pallas_call(
        finish_kernel,
        out_shape=jax.ShapeDtypeStruct((channels, seq_len), jnp.bfloat16),
        scratch_shapes=[
            pltpu.VMEM((2, heads, HEAD_DIM, HEAD_DIM), f32),
            pltpu.VMEM((blocks, heads, 2 * HEAD_DIM, HEAD_DIM), jnp.bfloat16),
        ],
        cost_estimate=pl.CostEstimate(
            flops=int(1e10 * heads * blocks / 32), bytes_accessed=1 << 23, transcendentals=1 << 14
        ),
        name="mixer_finish",
    )(gathered, steps, reads, local, mix_gain.reshape(channels, 1))


def slot_targets(routes, experts_n, capacity):
    onehot = (routes[:, :, None] == jnp.arange(experts_n, dtype=jnp.int32)[None, None, :]).astype(
        jnp.int32
    )
    flat = onehot.reshape(-1, experts_n)
    before = jnp.cumsum(flat, axis=0) - flat
    slot_index = jnp.sum(before * flat, axis=-1).reshape(routes.shape)
    return routes * capacity + slot_index


def dispatch_matrix(targets, slot_total):
    matches = targets[None, :, :] == jnp.arange(slot_total, dtype=jnp.int32)[:, None, None]
    return jnp.sum(matches.astype(jnp.float32), axis=-1).astype(jnp.bfloat16)


def expert_half(expert_in, expert_gain, routes, route_weight, gate_weight, up_weight, down_weight):
    experts_n = lax.axis_size("ep")
    row_count = expert_in.shape[0]
    capacity = 3 * routes.shape[1] * row_count // (2 * experts_n)
    slot_total = experts_n * capacity
    input_f = expert_in.astype(jnp.float32)
    normed = (
        input_f
        * lax.rsqrt(jnp.mean(input_f * input_f, axis=-1, keepdims=True) + 1e-06)
        * expert_gain
    ).astype(jnp.bfloat16)
    targets = slot_targets(routes, experts_n, capacity)
    buffer = jnp.dot(
        dispatch_matrix(targets, slot_total), normed, preferred_element_type=jnp.float32
    ).astype(jnp.bfloat16)
    gate_local = gate_weight[0]
    up_local = up_weight[0]
    down_local = down_weight[0]
    col_count = normed.shape[1] // lax.axis_size("tp")
    arrived = lax.all_to_all(
        buffer.reshape(experts_n, capacity, normed.shape[1]),
        "ep",
        split_axis=0,
        concat_axis=0,
        tiled=True,
    ).reshape(slot_total, normed.shape[1])
    gate_sum = jnp.dot(arrived, gate_local, preferred_element_type=jnp.float32)
    up_sum = jnp.dot(arrived, up_local, preferred_element_type=jnp.float32)
    hidden = (jax.nn.silu(gate_sum) * up_sum).astype(jnp.bfloat16)
    summed = lax.psum_scatter(
        lax.dot_general(
            down_local, hidden, (((0,), (1,)), ((), ())), preferred_element_type=jnp.float32
        ).astype(jnp.bfloat16),
        "tp",
        scatter_dimension=0,
        tiled=True,
    )
    returned = lax.all_to_all(
        summed.reshape(col_count, experts_n, capacity),
        "ep",
        split_axis=1,
        concat_axis=1,
        tiled=True,
    ).reshape(col_count, slot_total)
    matches = targets[:, :, None] == jnp.arange(slot_total, dtype=jnp.int32)[None, None, :]
    combine = jnp.sum(matches.astype(jnp.float32) * route_weight[:, :, None], axis=1)
    return jnp.einsum("tx,cx->tc", combine, returned.astype(jnp.float32), precision=highest).astype(
        jnp.bfloat16
    )


def on_device(
    query_in,
    key_in,
    value_in,
    erase_pre,
    decay_pre,
    mix_gain,
    expert_in,
    expert_gain,
    routes,
    route_weight,
    gate_weight,
    up_weight,
    down_weight,
):
    mixer_out = mixer_half(query_in, key_in, value_in, erase_pre, decay_pre, mix_gain)
    expert_out = expert_half(
        expert_in, expert_gain, routes, route_weight, gate_weight, up_weight, down_weight
    )
    return (mixer_out, expert_out)


def solution(mesh):
    placed = (
        P("tp", "ep"),
        P("tp", "ep"),
        P("tp", "ep"),
        P("tp", "ep"),
        P("tp", "ep"),
        P("tp"),
        P("ep", None),
        P(),
        P("ep", None),
        P("ep", None),
        P("ep", None, "tp"),
        P("ep", None, "tp"),
        P("ep", "tp", None),
    )
    return jax.shard_map(
        on_device,
        mesh=mesh,
        in_specs=placed,
        out_specs=(P("tp", "ep"), P("ep", "tp")),
        check_vma=False,
    )
```

time: 1450 us -> 207 us (0.14); the launches traced: 1430 us -> 207 us
  other arithmetic: 730 us -> 5.68 us
  matrix products: 384 us -> 20.8 us
  local copies, waits for them, and re-layouts: 225 us -> 2.44 us
  Pallas kernels: 0 us -> 53.5 us
  waiting for transfers between devices: 0.04 us -> 27 us
  blocking collectives: 63 us -> 77.9 us
    another operation x132 -> x2, other arithmetic: 698 us -> 1.18 us  [the longest x128 694 us: advance(): jax.scipy.linalg.solve_triangular(smat_b, right_side, lower=True, unit_di...]
    dot_general x250 -> x0, matrix products: 331 us -> none  [the longest x8 50.2 us: paired(): jnp.einsum('nthk,nshk->nhts', left, right, precision=highest)]
    dynamic_slice x96 -> x0, local copies, waits for them, and re-layouts: 87.7 us -> none  [the longest x64 79.2 us: run_blocks(): lax.scan(advance, initial, (unit_down, query_down, key_end, erase_end, au...]
    all_to_all x0 -> x1, blocking collectives: none -> 77.9 us  [expert_half(): lax.all_to_all(buffer.reshape(experts_n, capacity, normed.shape[1]), 'ep'...]
    all_gather x4 -> x0, blocking collectives: 63 us -> none  [prefix(): lax.all_gather(part.astype(kind), axis)]
    pallas_call x0 -> x2, Pallas kernels: none -> 53.5 us  [the longest x1 42.5 us: mixer_half(): pl.pallas_call(local_kernel, grid=(blocks,), in_specs=[taken] * 5, out_sp...]
    reshape x14 -> x1, local copies, waits for them, and re-layouts: 39 us -> 0.8 us  [mixer_half(): mix_gain.reshape(channels, 1)]
    another operation x32 -> x0, matrix products: 27 us -> none  [advance(): jax.scipy.linalg.solve_triangular(smat_b, right_side, lower=True, unit_di...]
  transfers between devices with their start and end apart: 3 -> 3, of which waited for: 0 -> 1; matrix products, arithmetic and copies ran while one was open for 91% -> 1% of each run, Pallas kernels for 0% -> 26%
where the time goes in v1:
time: 207 us
  blocking collectives  77.9 us (38%)
  Pallas kernels  53.5 us (26%)
  waiting for transfers between devices  27 us (13%)
  matrix products  20.8 us (10%)
  between operations  15.6 us (8%)
  other arithmetic  5.68 us (3%)
  starting transfers between devices  3.82 us (2%)
  local copies, waits for them, and re-layouts  2.44 us (1%)
    all_to_all x1, blocking collectives, expert_half(): lax.all_to_all(buffer.reshape(experts_n, capacity, normed.shape[1]), 'ep'...  77.9 us
    pallas_call x1, Pallas kernels, mixer_half(): pl.pallas_call(local_kernel, grid=(blocks,), in_specs=[taken] * 5, out_sp...  42.5 us
    all_gather x1, waiting for transfers between devices, mixer_half(): gathered = lax.all_gather(maps.astype(jnp.bfloat16), 'ep')  27 us
    dot_general x1, matrix products, expert_half(): lax.dot_general(down_local, hidden, (((0,), (1,)), ((), ())), preferred_e...  12.4 us
    pallas_call x1, Pallas kernels, mixer_half(): pl.pallas_call(finish_kernel, out_shape=jax.ShapeDtypeStruct((channels, s...  11 us
    dot_general x1, matrix products, expert_half(): up_sum = jnp.dot(arrived, up_local, preferred_element_type=jnp.float32)  5 us
  transfers between devices with their start and end apart: 3, of which 1 were waited for; matrix products, arithmetic and copies ran while one was open for 1% of the time, Pallas kernels for 26%

profile of v1, /device:TPU:0, one launch (start us, length us, event | category | flops | bytes accessed | tf_op | source)
XLA Modules:
  0.0 206.8 jit_solution(13481768282350965810)
XLA Ops:
  8.0 0.0 copy-start
  8.0 0.0 reduce-scatter.2.cloned.1.call-start
  8.1 0.9 copy.38
  8.9 0.1 eq.56
  9.1 0.1 eq.52
  9.3 1.1 reduce-window.6
  10.4 0.2 slice_reduce_fusion
  10.7 0.1 fusion.24
  10.7 0.1 reshape.54
  10.9 0.1 copy.40
  11.0 0.7 multiply_add_fusion
  11.7 0.3 convert_reduce_fusion
  12.0 1.5 fusion.12
  13.5 1.8 convolution_convert_fusion
  15.4 0.0 copy-start.3
  15.4 77.9 %all_to_all.10 = bf16[8,96,2048]{2,1,0:T(8,128)(2,1)S(1)} all-to-all(bf16[8,96,2048]{2,1,0:T(8,128)(2,1)S(1)} %bitcast.38), channel_id=1, replica_groups=mesh['ep'=8,'tp'=4] {'ep'}, dimensions={0} | all-to-all | bytes 6291456 | tf_op jit(solution)/shard_map/all_to_all | solution.py:278
  93.3 5.0 %fusion.2 = f32[768,896]{1,0:T(8,128)} fusion(bf16[768,2048]{1,0:T(8,128)(2,1)S(1)} %bitcast.40, bf16[1,2048,896]{2,1,0:T(8,128)(2,1)S(1)} %copy-done.3), kind=kOutput, calls=%fused_computation.2 | convolution fusion | flops 2818572288 | bytes 9568256 | tf_op jit(solution)/shard_map/dot_general | solution.py:286
  98.3 12.4 %fusion.9 = bf16[2048,768]{0,1:T(8,128)(2,1)} fusion(bf16[1,896,2048]{2,1,0:T(8,128)(2,1)} %param.25, f32[768,896]{1,0:T(8,128)} %fusion.2, bf16[768,2048]{1,0:T(8,128)(2,1)S(1)} %bitcast.41, bf16[1,2048,896]{2,1,0:T(8,128)(2,1)} %param.23), kind=kOutput, calls=%fused_computation.8 | convolution fusion | flops 5642846208 | bytes 16384000 | tf_op jit(solution)/shard_map/dot_general | solution.py:289
  110.7 0.0 reduce-scatter.2.cloned.1.call-update
  110.8 0.0 copy-start.2
  110.8 0.0 copy-start.1
  110.8 0.2 all-gather.3.cloned.1.call-start
  111.0 42.5 %mixer_local.1 = (bf16[2,256,1024]{2,1,0:T(8,128)(2,1)}, f32[256,1024]{1,0:T(8,128)}, f32[8,2,4,64,128]{4,3,2,1,0:T(8,128)}, f32[2,4,64,128]{3,2,1,0:T(8,128)}) custom-call(bf16[256,1024]{1,0:T(8,128)(2,1)} %q_ref.1, bf16[256,1024]{1,0:T(8,128)(2,1)} %k_ref.1, bf16[256,1024]{1,0:T(8,128)(2,1)} %v_ref.1, bf16[256,1024]{1,0:T(8,128)(2,1)} %e_ref.1, ...), custom_call_target="tpu_custom_call" | custom-call | flops 40000000000 | bytes 8388608 | tf_op jit(solution)/shard_map/mixer_local/pallas_call | solution.py:207
  153.5 1.6 convert_element_type.40
  155.1 0.0 all-gather.3.cloned.1.call-update
  155.2 0.0 reduce-scatter.2.cloned.1.call-done
  155.2 3.6 %all-to-all-start.1 = ((bf16[512,8,96]{0,2,1:T(8,128)(2,1)}), bf16[512,8,96]{0,2,1:T(8,128)(2,1)S(1)}, u32[]{:S(2)}, u32[]{:S(2)}) async-start(bf16[512,8,96]{0,2,1:T(8,128)(2,1)} %bitcast.42), calls=%async_computation.2 | async-start | bytes 1572864 | tf_op jit(solution)/shard_map/all_to_all | solution.py:296
  158.8 0.8 copy.37.gain_ref
  159.6 0.2 select_reduce_fusion
  159.8 27.0 %all-gather.3.cloned.1.call-done = bf16[16,4,64,128]{3,2,1,0:T(8,128)(2,1)} async-done(((bf16[2,4,64,128]{3,2,1,0:T(8,128)(2,1)}), bf16[16,4,64,128]{3,2,1,0:T(8,128)(2,1)}) %all-gather.3.cloned.1.call-update) | async-done | bytes 1048592 | tf_op jit(solution)/shard_map/all_gather | solution.py:229
  186.8 11.0 %mixer_finish.1 = bf16[256,1024]{1,0:T(8,128)(2,1)} custom-call(bf16[8,2,4,64,128]{4,3,2,1,0:T(8,128)(2,1)} %bitcast.44, f32[8,2,4,64,128]{4,3,2,1,0:T(8,128)} %get-tuple-element.7.step_ref, bf16[2,256,1024]{2,1,0:T(8,128)(2,1)} %get-tuple-element.8.read_ref, f32[256,1024]{1,0:T(8,128)} %get-tuple-element.9.local_ref, f32[256,1]{1,0:T(8,128)} %copy.37.gain_ref), custom_call_target="tpu_custom_call" | custom-call | flops 10000000000 | bytes 8388608 | tf_op jit(solution)/shard_map/mixer_finish/pallas_call | solution.py:230
  197.8 1.5 convolution_convert_fusion.1
  (9 shorter events, 0.1 us)
Async XLA Ops:
  8.0 5.5 %copy-start = (bf16[256,2048]{1,0:T(8,128)(2,1)S(1)}, bf16[256,2048]{1,0:T(8,128)(2,1)}, u32[]{:S(2)}) copy-start(bf16[256,2048]{1,0:T(8,128)(2,1)} %param.19) | copy-start | bytes 3145732
  8.0 147.2 %reduce-scatter.2.cloned.1.call-start = ((), (), s32[]{:S(2)}) async-start(), calls=%async_computation.3 | async-start | bytes 3932160 | tf_op jit(solution)/shard_map/reduce_scatter | solution.py:288
  15.4 77.9 %copy-start.3 = (bf16[1,2048,896]{2,1,0:T(8,128)(2,1)S(1)}, bf16[1,2048,896]{2,1,0:T(8,128)(2,1)}, u32[]{:S(2)}) copy-start(bf16[1,2048,896]{2,1,0:T(8,128)(2,1)} %param.24) | copy-start | bytes 11010052
  110.8 48.0 %copy-start.2 = (f32[256]{0:T(256)S(1)}, f32[256]{0:T(256)}, u32[]{:S(2)}) copy-start(f32[256]{0:T(256)} %param.18) | copy-start | bytes 3076
  110.8 48.8 %copy-start.1 = (f32[256,2]{0,1:T(2,128)S(1)}, f32[256,2]{0,1:T(2,128)}, u32[]{:S(2)}) copy-start(f32[256,2]{0,1:T(2,128)} %param.22) | copy-start | bytes 6148
  110.8 76.0 %all-gather.3.cloned.1.call-start = ((), (), s32[]{:S(2)}) async-start(), calls=%async_computation.4 | async-start | bytes 1179648 | tf_op jit(solution)/shard_map/all_gather | solution.py:229
  155.2 42.6 %all-to-all-start.1 = ((bf16[512,8,96]{0,2,1:T(8,128)(2,1)}), bf16[512,8,96]{0,2,1:T(8,128)(2,1)S(1)}, u32[]{:S(2)}, u32[]{:S(2)}) async-start(bf16[512,8,96]{0,2,1:T(8,128)(2,1)} %bitcast.42), calls=%async_computation.2 | async-start | bytes 1572864 | tf_op jit(solution)/shard_map/all_to_all | solution.py:296
Sparse Core Ops, SparseCore 0:
  110.9 42.9 reduce-scatter.1
Sparse Core Ops, SparseCore 1:
  155.2 31.5 all-gather.2

commit v2 on v1

--- a/solution.py
+++ b/solution.py
@@ -198,7 +198,7 @@
     lax.fori_loop(0, blocks, write, 0)
 
 
-def mixer_half(query_in, key_in, value_in, erase_pre, decay_pre, mix_gain):
+def mixer_local(query_in, key_in, value_in, erase_pre, decay_pre):
     channels, seq_len = query_in.shape
     heads = channels // HEAD_DIM
     blocks = seq_len // SPAN
@@ -226,7 +226,13 @@
         ),
         name="mixer_local",
     )(query_in, key_in, value_in, erase_pre, decay_pre)
-    gathered = lax.all_gather(maps.astype(jnp.bfloat16), "ep")
+    return reads, local, steps, maps
+
+
+def mixer_finish(gathered, steps, reads, local, mix_gain):
+    channels, seq_len = local.shape
+    blocks, _, heads = steps.shape[:3]
+    f32 = jnp.float32
     return pl.pallas_call(
         finish_kernel,
         out_shape=jax.ShapeDtypeStruct((channels, seq_len), jnp.bfloat16),
@@ -256,7 +262,9 @@
     return jnp.sum(matches.astype(jnp.float32), axis=-1).astype(jnp.bfloat16)
 
 
-def expert_half(expert_in, expert_gain, routes, route_weight, gate_weight, up_weight, down_weight):
+def expert_half(
+    hold, expert_in, expert_gain, routes, route_weight, gate_weight, up_weight, down_weight
+):
     experts_n = lax.axis_size("ep")
     row_count = expert_in.shape[0]
     capacity = 3 * routes.shape[1] * row_count // (2 * experts_n)
@@ -268,27 +276,32 @@
         * expert_gain
     ).astype(jnp.bfloat16)
     targets = slot_targets(routes, experts_n, capacity)
+    col_count = normed.shape[1] // lax.axis_size("tp")
+    mine = lax.dynamic_slice_in_dim(normed, lax.axis_index("tp") * col_count, col_count, 1)
     buffer = jnp.dot(
-        dispatch_matrix(targets, slot_total), normed, preferred_element_type=jnp.float32
+        dispatch_matrix(targets, slot_total), mine, preferred_element_type=jnp.float32
     ).astype(jnp.bfloat16)
     gate_local = gate_weight[0]
     up_local = up_weight[0]
     down_local = down_weight[0]
-    col_count = normed.shape[1] // lax.axis_size("tp")
-    arrived = lax.all_to_all(
-        buffer.reshape(experts_n, capacity, normed.shape[1]),
+    share = lax.all_to_all(
+        buffer.reshape(experts_n, capacity, col_count),
         "ep",
         split_axis=0,
         concat_axis=0,
         tiled=True,
-    ).reshape(slot_total, normed.shape[1])
+    ).reshape(slot_total, col_count)
+    arrived = lax.all_gather(share, "tp", axis=1, tiled=True)
+    arrived, gathered = hold(arrived)
     gate_sum = jnp.dot(arrived, gate_local, preferred_element_type=jnp.float32)
     up_sum = jnp.dot(arrived, up_local, preferred_element_type=jnp.float32)
     hidden = (jax.nn.silu(gate_sum) * up_sum).astype(jnp.bfloat16)
+    partial_sum = lax.dot_general(
+        down_local, hidden, (((0,), (1,)), ((), ())), preferred_element_type=jnp.float32
+    ).astype(jnp.bfloat16)
+    partial_sum, gathered = lax.optimization_barrier((partial_sum, gathered))
     summed = lax.psum_scatter(
-        lax.dot_general(
-            down_local, hidden, (((0,), (1,)), ((), ())), preferred_element_type=jnp.float32
-        ).astype(jnp.bfloat16),
+        partial_sum,
         "tp",
         scatter_dimension=0,
         tiled=True,
@@ -302,9 +315,10 @@
     ).reshape(col_count, slot_total)
     matches = targets[:, :, None] == jnp.arange(slot_total, dtype=jnp.int32)[None, None, :]
     combine = jnp.sum(matches.astype(jnp.float32) * route_weight[:, :, None], axis=1)
-    return jnp.einsum("tx,cx->tc", combine, returned.astype(jnp.float32), precision=highest).astype(
-        jnp.bfloat16
-    )
+    result = jnp.einsum(
+        "tx,cx->tc", combine, returned.astype(jnp.float32), precision=highest
+    ).astype(jnp.bfloat16)
+    return result, gathered
 
 
 def on_device(
@@ -322,10 +336,16 @@
     up_weight,
     down_weight,
 ):
-    mixer_out = mixer_half(query_in, key_in, value_in, erase_pre, decay_pre, mix_gain)
-    expert_out = expert_half(
-        expert_in, expert_gain, routes, route_weight, gate_weight, up_weight, down_weight
-    )
+    reads, local, steps, maps = mixer_local(query_in, key_in, value_in, erase_pre, decay_pre)
+
+    def hold(arrived):
+        held, sent = lax.optimization_barrier((arrived, maps.astype(jnp.bfloat16)))
+        return held, lax.all_gather(sent, "ep")
+
+    expert_out, gathered = expert_half(
+        hold, expert_in, expert_gain, routes, route_weight, gate_weight, up_weight, down_weight
+    )
+    mixer_out = mixer_finish(gathered, steps, reads, local, mix_gain)
     return (mixer_out, expert_out)
 
 

time: 207 us -> 189 us (0.913)
  blocking collectives: 77.9 us -> 27.2 us
  waiting for transfers between devices: 27 us -> 57.8 us
    all_to_all x1, blocking collectives: 77.9 us -> 27.2 us  [expert_half(): lax.all_to_all(buffer.reshape(experts_n, capacity, col_count), 'ep', spli...]
    reduce_scatter x1, waiting for transfers between devices: 0.02 us -> 46.5 us  [expert_half(): lax.psum_scatter(partial_sum, 'tp', scatter_dimension=0, tiled=True)]
    all_gather x1 -> x2, waiting for transfers between devices: 27 us -> 2.35 us  [the longest x1 2.35 us: hold(): return (held, lax.all_gather(sent, 'ep'))]
    all_to_all x1, waiting for transfers between devices: 0.01 us -> 8.89 us  [expert_half(): lax.all_to_all(summed.reshape(col_count, experts_n, capacity), 'ep', spli...]
    dot_general x1, matrix products: 5 us -> 8.11 us  [expert_half(): up_sum = jnp.dot(arrived, up_local, preferred_element_type=jnp.float32)]
  transfers between devices with their start and end apart: 3 -> 4, of which waited for: 1 -> 3; matrix products, arithmetic and copies ran while one was open for 1% -> 12% of each run, Pallas kernels for 26% -> 28%
where the time goes in v2:
time: 189 us; the launch traced here: 188 us
  waiting for transfers between devices  57.8 us (31%)
  Pallas kernels  53.5 us (28%)
  blocking collectives  27.2 us (14%)
  matrix products  22.5 us (12%)
  between operations  13.9 us (7%)
  other arithmetic  5.21 us (3%)
  starting transfers between devices  4.89 us (3%)
  local copies, waits for them, and re-layouts  3.2 us (2%)
    reduce_scatter x1, waiting for transfers between devices, expert_half(): lax.psum_scatter(partial_sum, 'tp', scatter_dimension=0, tiled=True)  46.5 us
    pallas_call x1, Pallas kernels, mixer_local(): pl.pallas_call(local_kernel, grid=(blocks,), in_specs=[taken] * 5, out_sp...  42.5 us
    all_to_all x1, blocking collectives, expert_half(): lax.all_to_all(buffer.reshape(experts_n, capacity, col_count), 'ep', spli...  27.2 us
    dot_general x1, matrix products, expert_half(): lax.dot_general(down_local, hidden, (((0,), (1,)), ((), ())), preferred_e...  12.5 us
    pallas_call x1, Pallas kernels, mixer_finish(): pl.pallas_call(finish_kernel, out_shape=jax.ShapeDtypeStruct((channels, s...  11 us
    all_to_all x1, waiting for transfers between devices, expert_half(): lax.all_to_all(summed.reshape(col_count, experts_n, capacity), 'ep', spli...  8.89 us
    dot_general x1, matrix products, expert_half(): up_sum = jnp.dot(arrived, up_local, preferred_element_type=jnp.float32)  8.11 us
    all_to_all x1, starting transfers between devices, expert_half(): lax.all_to_all(summed.reshape(col_count, experts_n, capacity), 'ep', spli...  4.59 us
  transfers between devices with their start and end apart: 4, of which 3 were waited for; matrix products, arithmetic and copies ran while one was open for 12% of the time, Pallas kernels for 28%

profile of v2, /device:TPU:0, one launch (start us, length us, event | category | flops | bytes accessed | tf_op | source)
XLA Modules:
  0.0 188.2 jit_solution(14446818803116518032)
XLA Ops:
  7.2 0.0 all-gather.4.cloned.1.call-start
  7.2 0.9 copy.37
  8.1 0.1 eq.56
  8.3 0.1 eq.52
  8.4 1.5 convert_element_type.44
  9.9 0.3 multiply_reduce_fusion
  10.2 1.1 reduce-window.6
  11.3 0.2 slice_reduce_fusion
  11.6 0.1 fusion.23
  11.7 0.1 reshape.53
  11.8 0.1 copy.39
  11.9 0.3 convert_reduce_fusion
  12.3 0.8 dynamic-slice
  13.1 0.4 convolution_convert_fusion
  13.5 27.2 %all_to_all.10 = bf16[8,96,512]{2,1,0:T(8,128)(2,1)} all-to-all(bf16[8,96,512]{2,1,0:T(8,128)(2,1)S(1)} %bitcast.40), channel_id=1, replica_groups=mesh['ep'=8,'tp'=4] {'ep'}, dimensions={0} | all-to-all | bytes 1572864 | tf_op jit(solution)/shard_map/all_to_all | solution.py:287
  40.7 0.0 all-gather.4.cloned.1.call-update
  40.7 0.0 all-gather.6.cloned.1.call-start
  40.8 42.5 %mixer_local.1 = (bf16[2,256,1024]{2,1,0:T(8,128)(2,1)}, f32[256,1024]{1,0:T(8,128)}, f32[8,2,4,64,128]{4,3,2,1,0:T(8,128)}, f32[2,4,64,128]{3,2,1,0:T(8,128)}) custom-call(bf16[256,1024]{1,0:T(8,128)(2,1)} %q_ref.1, bf16[256,1024]{1,0:T(8,128)(2,1)} %k_ref.1, bf16[256,1024]{1,0:T(8,128)(2,1)} %v_ref.1, bf16[256,1024]{1,0:T(8,128)(2,1)} %e_ref.1, ...), custom_call_target="tpu_custom_call" | custom-call | flops 40000000000 | bytes 8388608 | tf_op jit(solution)/shard_map/mixer_local/pallas_call | solution.py:207
  83.3 1.6 convert_element_type.47
  84.9 0.0 all-gather.6.cloned.1.call-update
  84.9 0.2 reduce-scatter.2.cloned.1.call-start
  85.2 8.1 %fusion.2 = f32[768,896]{1,0:T(8,128)} fusion(bf16[768,2048]{1,0:T(8,128)(2,1)} %all-gather.4.cloned.1.call-done, bf16[1,2048,896]{2,1,0:T(8,128)(2,1)} %param.24), kind=kOutput, calls=%fused_computation.2 | convolution fusion | flops 2818572288 | bytes 9568256 | tf_op jit(solution)/shard_map/dot_general | solution.py:297
  93.3 12.5 %fusion.9 = bf16[2048,768]{0,1:T(8,128)(2,1)} fusion(bf16[1,896,2048]{2,1,0:T(8,128)(2,1)} %param.25, f32[768,896]{1,0:T(8,128)} %fusion.2, bf16[768,2048]{1,0:T(8,128)(2,1)S(1)} %copy-done.4, bf16[1,2048,896]{2,1,0:T(8,128)(2,1)} %param.23), kind=kOutput, calls=%fused_computation.7 | convolution fusion | flops 5642846208 | bytes 16384000 | tf_op jit(solution)/shard_map/dot_general | solution.py:299
  105.7 2.4 %all-gather.6.cloned.1.call-done = bf16[16,4,64,128]{3,2,1,0:T(8,128)(2,1)} async-done(((bf16[2,4,64,128]{3,2,1,0:T(8,128)(2,1)}), bf16[16,4,64,128]{3,2,1,0:T(8,128)(2,1)}) %all-gather.6.cloned.1.call-update) | async-done | bytes 1048592 | tf_op jit(solution)/shard_map/all_gather | solution.py:343
  108.1 0.0 reduce-scatter.2.cloned.1.call-update
  108.1 46.5 %reduce-scatter.2.cloned.1.call-done = bf16[512,768]{0,1:T(8,128)(2,1)} async-done(((bf16[2048,768]{0,1:T(8,128)(2,1)}), bf16[512,768]{0,1:T(8,128)(2,1)}) %reduce-scatter.2.cloned.1.call-update) | async-done | bytes 786448 | tf_op jit(solution)/shard_map/reduce_scatter | solution.py:303
  154.6 4.6 %all-to-all-start.1 = ((bf16[512,8,96]{0,2,1:T(8,128)(2,1)}), bf16[512,8,96]{0,2,1:T(8,128)(2,1)S(1)}, u32[]{:S(2)}, u32[]{:S(2)}) async-start(bf16[512,8,96]{0,2,1:T(8,128)(2,1)} %bitcast.41), calls=%async_computation.2 | async-start | bytes 1572864 | tf_op jit(solution)/shard_map/all_to_all | solution.py:309
  159.2 0.8 copy.40.gain_ref
  160.0 0.2 select_reduce_fusion
  160.2 11.0 %mixer_finish.1 = bf16[256,1024]{1,0:T(8,128)(2,1)} custom-call(bf16[8,2,4,64,128]{4,3,2,1,0:T(8,128)(2,1)} %bitcast.43, f32[8,2,4,64,128]{4,3,2,1,0:T(8,128)} %get-tuple-element.14.step_ref, bf16[2,256,1024]{2,1,0:T(8,128)(2,1)} %get-tuple-element.15.read_ref, f32[256,1024]{1,0:T(8,128)} %get-tuple-element.16.local_ref, f32[256,1]{1,0:T(8,128)} %copy.40.gain_ref), custom_call_target="tpu_custom_call" | custom-call | flops 10000000000 | bytes 8388608 | tf_op jit(solution)/shard_map/mixer_finish/pallas_call | solution.py:236
  171.3 8.9 %all-to-all-done.1 = bf16[512,8,96]{0,2,1:T(8,128)(2,1)S(1)} async-done(((bf16[512,8,96]{0,2,1:T(8,128)(2,1)}), bf16[512,8,96]{0,2,1:T(8,128)(2,1)S(1)}, u32[]{:S(2)}, u32[]{:S(2)}) %all-to-all-start.1) | async-done | bytes 786464 | tf_op jit(solution)/shard_map/all_to_all | solution.py:309
  180.2 1.5 convolution_convert_fusion.1
  (16 shorter events, 0.1 us)
Async XLA Ops:
  7.2 4.8 %copy-start.1 = (s32[256,2]{0,1:T(2,128)S(1)}, s32[256,2]{0,1:T(2,128)}, u32[]{:S(2)}) copy-start(s32[256,2]{0,1:T(2,128)} %param.21) | copy-start | bytes 6148
  7.2 2.7 %copy-start = (bf16[256,2048]{1,0:T(8,128)(2,1)S(1)}, bf16[256,2048]{1,0:T(8,128)(2,1)}, u32[]{:S(2)}) copy-start(bf16[256,2048]{1,0:T(8,128)(2,1)} %param.19) | copy-start | bytes 3145732
  7.2 77.7 %all-gather.4.cloned.1.call-start = ((), (), s32[]{:S(2)}) async-start(), calls=%async_computation.3 | async-start | bytes 3932160 | tf_op jit(solution)/shard_map/all_gather | solution.py:294
  40.7 67.3 %all-gather.6.cloned.1.call-start = ((), (), s32[]{:S(2)}) async-start(), calls=%async_computation.5 | async-start | bytes 1179648 | tf_op jit(solution)/shard_map/all_gather | solution.py:343
  84.9 8.3 %copy-start.4 = (bf16[768,2048]{1,0:T(8,128)(2,1)S(1)}, bf16[768,2048]{1,0:T(8,128)(2,1)}, u32[]{:S(2)}) copy-start(bf16[768,2048]{1,0:T(8,128)(2,1)} %all-gather.4.cloned.1.call-done) | copy-start | bytes 9437188
  84.9 69.7 %reduce-scatter.2.cloned.1.call-start = ((), (), s32[]{:S(2)}) async-start(), calls=%async_computation.4 | async-start | bytes 3932160 | tf_op jit(solution)/shard_map/reduce_scatter | solution.py:303
  105.7 53.5 %copy-start.3 = (f32[256]{0:T(256)S(1)}, f32[256]{0:T(256)}, u32[]{:S(2)}) copy-start(f32[256]{0:T(256)} %param.18) | copy-start | bytes 3076
  105.7 54.3 %copy-start.2 = (f32[256,2]{0,1:T(2,128)S(1)}, f32[256,2]{0,1:T(2,128)}, u32[]{:S(2)}) copy-start(f32[256,2]{0,1:T(2,128)} %param.22) | copy-start | bytes 6148
  154.6 25.5 %all-to-all-start.1 = ((bf16[512,8,96]{0,2,1:T(8,128)(2,1)}), bf16[512,8,96]{0,2,1:T(8,128)(2,1)S(1)}, u32[]{:S(2)}, u32[]{:S(2)}) async-start(bf16[512,8,96]{0,2,1:T(8,128)(2,1)} %bitcast.41), calls=%async_computation.2 | async-start | bytes 1572864 | tf_op jit(solution)/shard_map/all_to_all | solution.py:309
Sparse Core Ops, SparseCore 0:
  40.8 42.7 all-gather.3
  85.8 22.2 all-gather.5
  111.1 43.5 reduce-scatter.1
